TPU v7x, 128 devices: a whole 4x4x4 slice. The times are simulated.
128 devices in a mesh: sp: 32 (over z, y, core), tp: 4 (over x).
Axes of the slice: x: 4, y: 4, z: 4, core: 2. Of those that a mesh axis runs over, the one named last changes fastest.
Arguments:
- residual_in: bfloat16 [32768, 2048], P(('sp', 'tp')), may hold values from -6 to 6
- queries: bfloat16 [32768, 2048], P('sp', 'tp'), may hold values from -200 to 200, as said below
- keys_values: bfloat16 [2, 32768, 1024], P(None, 'sp', 'tp'), may hold values from -6 to 6
- sink_logit: float32 [32], P('tp'), may hold values from -2 to 6
- out_weight: bfloat16 [2048, 2048], P('tp'), may hold values from -2 to 2
- norm1_gain: float32 [2048], replicated, may hold values from 0.1 to 1.9
- norm1_bias: float32 [2048], replicated, may hold values from -3 to 3
- up_weight: bfloat16 [2048, 8192], P('sp', 'tp'), may hold values from -0.125 to 0.125
- down_weight: bfloat16 [8192, 2048], P('tp', 'sp'), may hold values from -0.0625 to 0.0625
- norm2_gain: float32 [2048], replicated, may hold values from 0.1 to 1.9
- norm2_bias: float32 [2048], replicated, may hold values from -3 to 3
Outputs:
- stream_out: bfloat16 [32768, 2048], P(('sp', 'tp'))
Inputs may be any that keep to these rules, and one draw needn't show every extreme that they name: `queries`: of order one mostly; some rows may be large multiples of a nearby key row.
All inputs are finite; a program needn't handle non-finite values.
Results may differ from a plain program's by a relative error of at most 0.014.
Values may be sent and summed in bfloat16 or wider, within the bound.
A program may use at most 128 MiB of HBM per device.

v0:
```python
import jax
import jax.numpy as jnp
from jax import lax
from jax.sharding import PartitionSpec as P

HEAD_DIM = 64
WINDOW = 128


def in_order(pieces, dim):
    dims = list(pieces.shape[1:])
    dims[dim] *= pieces.shape[0]
    return jnp.moveaxis(pieces, 0, dim).reshape(dims)


def one_gather(arrays, axis, dims):
    flat = jnp.concatenate([a.reshape(-1) for a in arrays])
    lines, at, finished = (lax.all_gather(flat, axis), 0, [])
    for a, dim in zip(arrays, dims):
        pieces = lines[:, at : at + a.size].reshape(-1, *a.shape)
        finished.append(in_order(pieces, dim))
        at += a.size
    return tuple(finished)


def with_halo(shard, sides, width):
    for axis, dim in sides:
        devices, length = (lax.axis_size(axis), shard.shape[dim])
        up = [(i, (i + 1) % devices) for i in range(devices - 1)]
        down = [(j, i) for i, j in up]
        last = lax.slice_in_dim(shard, length - width, length, axis=dim)
        first = lax.slice_in_dim(shard, 0, width, axis=dim)
        before = lax.ppermute(last, axis, up)
        after = lax.ppermute(first, axis, down)
        shard = jnp.concatenate([before, shard, after], axis=dim)
    return shard


def in_blocks(shard, dim, devices):
    dims = shard.shape
    pieces = shard.reshape(*dims[:dim], devices, dims[dim] // devices, *dims[dim + 1 :])
    return jnp.moveaxis(pieces, dim, 0)


def sent_and_summed(shard, axis, dim):
    pieces = in_blocks(shard, dim, lax.axis_size(axis))
    arrived = lax.all_to_all(pieces, axis, split_axis=0, concat_axis=0, tiled=True)
    return arrived.astype(jnp.float32).sum(axis=0)


def sent_to_all(shard, axis):
    devices = lax.axis_size(axis)
    return lax.all_to_all(
        jnp.broadcast_to(shard[None], (devices, *shard.shape)), axis, 0, 0, tiled=True
    )


def gathered_copies(shard, axis, dim):
    pieces = sent_to_all(shard, axis)
    return in_order(pieces, dim)


def norm_rows(values, gain, bias):
    mean = jnp.mean(values, axis=-1, keepdims=True)
    centred = values - mean
    variance = jnp.mean(centred * centred, axis=-1, keepdims=True)
    return (centred * lax.rsqrt(variance + 1e-06) * gain + bias).astype(jnp.bfloat16)


def attend(queries, padded, sink_logit, offset, total):
    tok_rows = queries.shape[0]
    block = min(512, tok_rows)
    span = block + 2 * WINDOW
    kv_local = padded.shape[2] // HEAD_DIM
    heads_local = queries.shape[1] // HEAD_DIM
    group = heads_local // kv_local
    sink = sink_logit.reshape(kv_local, group, 1, 1)

    def one_block(index):
        start = index * block
        query = lax.dynamic_slice_in_dim(queries, start, block, 0).reshape(
            block, kv_local, group, HEAD_DIM
        )
        keys = lax.dynamic_slice_in_dim(padded[0], start, span, 0).reshape(span, kv_local, HEAD_DIM)
        values = lax.dynamic_slice_in_dim(padded[1], start, span, 0).reshape(
            span, kv_local, HEAD_DIM
        )
        scores = jnp.einsum(
            "qhgd,khd->hgqk", query, keys, preferred_element_type=jnp.float32
        ) * HEAD_DIM ** (-0.5)
        query_pos = offset + start + jnp.arange(block, dtype=jnp.int32)
        key_pos = offset + start - WINDOW + jnp.arange(span, dtype=jnp.int32)
        valid = (
            (jnp.abs(key_pos[None, :] - query_pos[:, None]) <= WINDOW)
            & (key_pos[None, :] >= 0)
            & (key_pos[None, :] < total)
        )
        scores = jnp.where(valid, scores, -jnp.inf)
        top = jnp.maximum(jnp.max(scores, axis=-1, keepdims=True), sink)
        expd = jnp.exp(scores - top)
        denom = jnp.sum(expd, axis=-1, keepdims=True) + jnp.exp(sink - top)
        weights = (expd / denom).astype(jnp.bfloat16)
        mixed = jnp.einsum("hgqk,khd->qhgd", weights, values, preferred_element_type=jnp.float32)
        return mixed.reshape(block, heads_local * HEAD_DIM).astype(jnp.bfloat16)

    blocks = lax.map(one_block, jnp.arange(tok_rows // block, dtype=jnp.int32))
    return blocks.reshape(tok_rows, heads_local * HEAD_DIM)


def activate(rows, up_full):
    hidden = jnp.dot(rows, up_full, preferred_element_type=jnp.float32)
    return jnp.square(jnp.maximum(hidden, 0.0)).astype(jnp.bfloat16)


def on_device(
    residual_in,
    queries,
    keys_values,
    sink_logit,
    out_weight,
    norm1_gain,
    norm1_bias,
    up_weight,
    down_weight,
    norm2_gain,
    norm2_bias,
):
    up_full, down_full = one_gather((up_weight, down_weight), "sp", (0, 1))
    tok_rows = queries.shape[0]
    padded = with_halo(keys_values, (("sp", 1),), WINDOW)
    offset = lax.axis_index("sp") * tok_rows
    attended = attend(queries, padded, sink_logit, offset, tok_rows * lax.axis_size("sp"))
    rows = attended
    projected = sent_and_summed(
        jnp.dot(rows, out_weight, preferred_element_type=jnp.float32)
        .astype(jnp.bfloat16)
        .astype(jnp.float32)
        .astype(jnp.bfloat16),
        "tp",
        0,
    )
    first = norm_rows(residual_in.astype(jnp.float32) + projected, norm1_gain, norm1_bias)
    activation = activate(gathered_copies(first, "tp", 0), up_full)
    rows = activation
    branch = lax.psum_scatter(
        jnp.dot(rows, down_full, preferred_element_type=jnp.float32)
        .astype(jnp.bfloat16)
        .astype(jnp.float32)
        .astype(jnp.bfloat16),
        "tp",
        scatter_dimension=0,
        tiled=True,
    ).astype(jnp.float32)
    return norm_rows(first.astype(jnp.float32) + branch, norm2_gain, norm2_bias)


def solution(mesh):
    return jax.shard_map(
        on_device,
        mesh=mesh,
        in_specs=(
            P(("sp", "tp"), None),
            P("sp", "tp"),
            P(None, "sp", "tp"),
            P("tp"),
            P("tp", None),
            P(),
            P(),
            P("sp", "tp"),
            P("tp", "sp"),
            P(),
            P(),
        ),
        out_specs=P(("sp", "tp"), None),
        check_vma=False,
    )
```

profile of v0, /device:TPU:1, one launch (start us, length us, event | category | flops | bytes accessed | tf_op | source)
XLA Modules:
  0.0 300.6 jit_solution(18373947099800134417)
XLA Ops:
  6.5 1.4 copy.37
  7.9 0.3 reshape.135
  8.2 1.0 copy.45
  9.2 0.8 pad_maximum_fusion.1
  10.0 1.5 copy.31
  11.5 0.7 fusion.16
  12.2 3.3 %collective-permute-start.1 = (bf16[2,128,256]{1,2,0:T(8,128)(2,1)}, bf16[2,128,256]{1,2,0:T(8,128)(2,1)S(1)}, u32[]{:S(2)}, u32[]{:S(2)}) collective-permute-start(bf16[2,128,256]{1,2,0:T(8,128)(2,1)} %get-tuple-element.141), channel_id=1, source_target_pairs={{4,0},{8,4},{12,8},{16,12},{20,16},{24,20},{28,24},{32,28},{36,32}... | collective-permute-start | bytes 393224 | tf_op jit(solution)/shard_map/ppermute | solution.py:34
  15.5 3.2 %collective-permute-start = (bf16[2,128,256]{1,2,0:T(8,128)(2,1)S(1)}, bf16[2,128,256]{1,2,0:T(8,128)(2,1)S(1)}, u32[]{:S(2)}, u32[]{:S(2)}) collective-permute-start(bf16[2,128,256]{1,2,0:T(8,128)(2,1)S(1)} %get-tuple-element.140), channel_id=1, source_target_pairs={{0,4},{4,8},{8,12},{12,16},{16,20},{20,24},{24,28},{28,32},{32,36}... | collective-permute-start | bytes 393224 | tf_op jit(solution)/shard_map/ppermute | solution.py:33
  18.7 0.1 reshape.130
  18.8 0.1 copy.35
  18.9 0.7 collective-permute-done.1
  19.6 1.0 collective-permute-done
  20.7 1.2 pad_maximum_fusion
  21.8 53.7 %while.12 = (s32[]{:T(128)}, bf16[2,512,512]{2,1,0:T(8,128)(2,1)}, bf16[2,1280,256]{1,2,0:T(8,128)(2,1)}, s32[2]{0:T(128)S(1)}, s32[]{:T(128)}, /*index=5*/bf16[...) while((s32[]{:T(128)}, bf16[2,512,512]{2,1,0:T(8,128)(2,1)}, ...), condition=%wide.region_3.4_spmd, body=%wide.region_0.3_spmd.sunk | while | flops 845295104 | bytes 101627328 | solution.py:106
  21.8 1.5 fusion.37
  23.3 0.6 dynamic_slice.27
  24.6 1.0 constant_dynamic-slice_fusion.5
  25.5 0.8 fusion.39
  26.3 1.1 constant_dynamic-slice_fusion.6
  27.4 0.2 copy.49
  27.6 7.7 %fusion.40 = (f32[4,2,512]{2,1,0:T(2,128)S(1)}, f32[4,768,512,2]{2,1,3,0:T(8,128)}) fusion(pred[512,768]{0,1:T(8,128)(4,1)S(1)} %fusion.39, bf16[768,4,64,1]{0,2,3,1:T(8,128)(2,1)} %bitcast.68, bf16[512,4,2,64]{0,3,2,1:T(8,128)(2,1)S(1)} %bitcast.67), kind=kOutput, calls=%fused_computation.4.clone.1 | convolution fusion | flops 412086272 | bytes 13910016 | tf_op jit(solution)/shard_map/while/body/eval_jaxpr/qhgd,khd->hgqk/dot_general | solution.py:88
  35.3 0.1 copy.50
  35.4 0.1 broadcast_maximum_fusion.2
  35.5 7.3 %fusion.41 = f32[4,2,512]{2,1,0:T(2,128)S(1)} fusion(f32[4,768,512,2]{2,1,3,0:T(8,128)} %get-tuple-element.199, f32[4,2,512]{2,1,0:T(2,128)S(1)} %broadcast_maximum_fusion.2, pred[512,768]{0,1:T(8,128)(4,1)S(1)} %fusion.39), kind=kLoop, calls=%fused_computation.3.clone.1 | loop fusion | flops 12578816 | bytes 13008896 | tf_op jit(solution)/shard_map/while/body/eval_jaxpr/reduce_sum | solution.py:101
  42.8 0.1 exponential_add_fusion.2
  42.9 0.7 copy-done.1
  43.6 3.6 %fusion.42 = bf16[4,64,2,512]{3,1,2,0:T(8,128)(2,1)S(1)} fusion(bf16[768,4,64,1]{0,2,3,1:T(8,128)(2,1)S(1)} %bitcast.70, f32[4,768,512,2]{2,1,3,0:T(8,128)S(1)} %copy-done.1, f32[4,2,512]{2,1,0:T(2,128)S(1)} %exponential_add_fusion.2, f32[4,2,512]{2,1,0:T(2,128)S(1)} %broadcast_maximum_fusion.2, pred[512,768]{0,1:T(8,128)(4,1)S(1)} %fusion.39), kind=kOutput, calls=%fused_computation.9.clone.1 | convolution fusion | flops 418643968 | bytes 13926400 | tf_op jit(solution)/shard_map/while/body/eval_jaxpr/hgqk,khd->qhgd/dot_general | solution.py:103
  47.2 0.2 copy.51
  47.4 0.8 constant_dynamic-update-slice_fusion.2
  48.3 1.4 fusion.37
  49.6 0.6 dynamic_slice.27
  50.9 1.0 constant_dynamic-slice_fusion.5
  51.9 0.8 fusion.39
  52.7 1.1 constant_dynamic-slice_fusion.6
  53.8 0.2 copy.49
  54.0 7.7 %fusion.40 = (f32[4,2,512]{2,1,0:T(2,128)S(1)}, f32[4,768,512,2]{2,1,3,0:T(8,128)}) fusion(pred[512,768]{0,1:T(8,128)(4,1)S(1)} %fusion.39, bf16[768,4,64,1]{0,2,3,1:T(8,128)(2,1)} %bitcast.68, bf16[512,4,2,64]{0,3,2,1:T(8,128)(2,1)S(1)} %bitcast.67), kind=kOutput, calls=%fused_computation.4.clone.1 | convolution fusion | flops 412086272 | bytes 13910016 | tf_op jit(solution)/shard_map/while/body/eval_jaxpr/qhgd,khd->hgqk/dot_general | solution.py:88
  61.7 0.1 copy.50
  61.8 0.1 broadcast_maximum_fusion.2
  61.8 7.8 %fusion.41 = f32[4,2,512]{2,1,0:T(2,128)S(1)} fusion(f32[4,768,512,2]{2,1,3,0:T(8,128)} %get-tuple-element.199, f32[4,2,512]{2,1,0:T(2,128)S(1)} %broadcast_maximum_fusion.2, pred[512,768]{0,1:T(8,128)(4,1)S(1)} %fusion.39), kind=kLoop, calls=%fused_computation.3.clone.1 | loop fusion | flops 12578816 | bytes 13008896 | tf_op jit(solution)/shard_map/while/body/eval_jaxpr/reduce_sum | solution.py:101
  69.6 0.1 exponential_add_fusion.2
  69.7 1.1 copy-done.1
  70.9 3.6 %fusion.42 = bf16[4,64,2,512]{3,1,2,0:T(8,128)(2,1)S(1)} fusion(bf16[768,4,64,1]{0,2,3,1:T(8,128)(2,1)S(1)} %bitcast.70, f32[4,768,512,2]{2,1,3,0:T(8,128)S(1)} %copy-done.1, f32[4,2,512]{2,1,0:T(2,128)S(1)} %exponential_add_fusion.2, f32[4,2,512]{2,1,0:T(2,128)S(1)} %broadcast_maximum_fusion.2, pred[512,768]{0,1:T(8,128)(4,1)S(1)} %fusion.39), kind=kOutput, calls=%fused_computation.9.clone.1 | convolution fusion | flops 418643968 | bytes 13926400 | tf_op jit(solution)/shard_map/while/body/eval_jaxpr/hgqk,khd->qhgd/dot_general | solution.py:103
  74.5 0.2 copy.51
  74.7 0.8 constant_dynamic-update-slice_fusion.2
  75.5 3.7 %convolution_convert_fusion.1 = bf16[1024,2048]{1,0:T(8,128)(2,1)S(1)} fusion(bf16[1024,512]{1,0:T(8,128)(2,1)} %bitcast.76, bf16[512,2048]{1,0:T(8,128)(2,1)S(1)} %copy-done), kind=kOutput, calls=%fused_computation.25 | convolution fusion | flops 2149580800 | bytes 7340032 | tf_op jit(solution)/shard_map/dot_general | solution.py:135
  79.2 52.5 %all_to_all.10 = bf16[4,256,2048]{2,1,0:T(8,128)(2,1)S(1)} all-to-all(bf16[4,256,2048]{2,1,0:T(8,128)(2,1)S(1)} %bitcast.72), channel_id=1, replica_groups=mesh['sp'=32,'tp'=4] {'tp'}, dimensions={0} | all-to-all | bytes 8388608 | tf_op jit(solution)/shard_map/all_to_all | solution.py:47
  131.8 0.8 convert_reduce_fusion
  132.6 0.4 copy-done.4
  133.0 0.3 fusion.12
  133.3 0.5 multiply_reduce_fusion.1
  133.8 0.5 add_convert_fusion.1
  134.3 2.5 broadcast_in_dim.27
  136.9 4.8 %all-to-all-start.1 = ((bf16[4,256,2048]{2,1,0:T(8,128)(2,1)}), bf16[4,256,2048]{2,1,0:T(8,128)(2,1)}, u32[]{:S(2)}, u32[]{:S(2)}) async-start(bf16[4,256,2048]{2,1,0:T(8,128)(2,1)} %broadcast_in_dim.27), calls=%async_computation.1 | async-start | bytes 8388608 | tf_op jit(solution)/shard_map/all_to_all | solution.py:53
  141.7 0.0 reduce-scatter.2.cloned.1.call-start
  141.8 14.6 %reshape.138 = bf16[32,262144]{1,0:T(8,128)(2,1)} reshape(bf16[8388608]{0:T(1024)(128)(2,1)} %all-gather.3.cloned.1.call-done) | data formatting | bytes 33554432 | tf_op jit(solution)/shard_map/all_gather | solution.py:18
  156.3 11.3 %fusion.15 = (bf16[32,131072]{1,0:T(8,128)(2,1)}, bf16[32,131072]{1,0:T(8,128)(2,1)}) fusion(bf16[32,262144]{1,0:T(8,128)(2,1)} %reshape.138), kind=kLoop, calls=%fused_computation.43 | loop fusion | bytes 33554432 | tf_op jit(solution)/shard_map/slice | solution.py:20
  167.6 19.0 %reshape.136 = bf16[32,2048,64]{2,1,0:T(8,128)(2,1)} reshape(bf16[32,131072]{1,0:T(8,128)(2,1)} %get-tuple-element.139) | data formatting | bytes 16777216 | tf_op jit(solution)/shard_map/reshape | solution.py:20
  186.6 15.8 %copy.38 = bf16[2048,32,64]{0,2,1:T(8,128)(2,1)} copy(bf16[2048,32,64]{2,0,1:T(8,128)(2,1)} %bitcast.66) | data formatting | bytes 16777216 | tf_op jit(solution)/shard_map/transpose | solution.py:13
  202.4 8.9 %reshape_reshape.3 = bf16[2048,2048]{1,0:T(8,128)(2,1)} reshape(bf16[32,131072]{1,0:T(8,128)(2,1)} %get-tuple-element.138) | data formatting | bytes 16777216 | tf_op jit(solution)/shard_map/reshape;reshape | solution.py:13
  211.3 25.7 %convolution_convert_fusion = bf16[1024,2048]{1,0:T(8,128)(2,1)} fusion(bf16[2048,2048]{0,1:T(8,128)(2,1)} %bitcast.71, bf16[1024,2048]{1,0:T(8,128)(2,1)} %bitcast.14, bf16[2048,2048]{1,0:T(8,128)(2,1)} %reshape_reshape.3), kind=kOutput, calls=%fused_computation.24 | convolution fusion | flops 17188257792 | bytes 25165824 | tf_op jit(solution)/shard_map/dot_general | solution.py:146
  237.0 51.8 %reduce-scatter.2.cloned.1.call-done = bf16[256,2048]{1,0:T(8,128)(2,1)} async-done(((bf16[1024,2048]{1,0:T(8,128)(2,1)}), bf16[256,2048]{1,0:T(8,128)(2,1)}) %reduce-scatter.2.cloned.1.call-update) | async-done | bytes 1048592 | tf_op jit(solution)/shard_map/reduce_scatter | solution.py:145
  288.8 1.7 fusion.11
  290.5 1.7 multiply_reduce_fusion
  292.2 1.5 add_convert_fusion
  (38 shorter events, 0.2 us)
Async XLA Ops:
  6.5 69.0 %copy-start = (bf16[512,2048]{1,0:T(8,128)(2,1)S(1)}, bf16[512,2048]{1,0:T(8,128)(2,1)}, u32[]{:S(2)}) copy-start(bf16[512,2048]{1,0:T(8,128)(2,1)} %param.17) | copy-start | bytes 6291460
  6.5 12.2 %copy-start.9 = (f32[8]{0:T(128)S(1)}, f32[8]{0:T(128)}, u32[]{:S(2)}) copy-start(f32[8]{0:T(128)} %param.16) | copy-start | bytes 100
  6.5 135.2 %all-gather.3.cloned.1.call-start = ((), (), s32[]{:S(2)}) async-start(), calls=%async_computation.4 | async-start | bytes 17301504 | tf_op jit(solution)/shard_map/all_gather | solution.py:18
  12.2 7.4 %collective-permute-start.1 = (bf16[2,128,256]{1,2,0:T(8,128)(2,1)}, bf16[2,128,256]{1,2,0:T(8,128)(2,1)S(1)}, u32[]{:S(2)}, u32[]{:S(2)}) collective-permute-start(bf16[2,128,256]{1,2,0:T(8,128)(2,1)} %get-tuple-element.141), channel_id=1, source_target_pairs={{4,0},{8,4},{12,8},{16,12},{20,16},{24,20},{28,24},{32,28},{36,32}... | collective-permute-start | bytes 393224 | tf_op jit(solution)/shard_map/ppermute | solution.py:34
  15.5 5.1 %collective-permute-start = (bf16[2,128,256]{1,2,0:T(8,128)(2,1)S(1)}, bf16[2,128,256]{1,2,0:T(8,128)(2,1)S(1)}, u32[]{:S(2)}, u32[]{:S(2)}) collective-permute-start(bf16[2,128,256]{1,2,0:T(8,128)(2,1)S(1)} %get-tuple-element.140), channel_id=1, source_target_pairs={{0,4},{4,8},{8,12},{12,16},{16,20},{20,24},{24,28},{28,32},{32,36}... | collective-permute-start | bytes 393224 | tf_op jit(solution)/shard_map/ppermute | solution.py:33
  35.5 8.2 %copy-start.1 = (f32[4,768,512,2]{2,1,3,0:T(8,128)S(1)}, f32[4,768,512,2]{2,1,3,0:T(8,128)}, u32[]{:S(2)}) copy-start(f32[4,768,512,2]{2,1,3,0:T(8,128)} %get-tuple-element.199) | copy-start | bytes 37748740 | tf_op jit(solution)/shard_map/while
  35.5 8.2 %copy-start.2 = (bf16[1,768,256]{1,2,0:T(8,128)(2,1)S(1)}, bf16[1,768,256]{1,2,0:T(8,128)(2,1)}, u32[]{:S(2)}) copy-start(bf16[1,768,256]{1,2,0:T(8,128)(2,1)} %get-tuple-element.195) | copy-start | bytes 1179652 | tf_op jit(solution)/shard_map/while
  61.8 9.0 %copy-start.1 = (f32[4,768,512,2]{2,1,3,0:T(8,128)S(1)}, f32[4,768,512,2]{2,1,3,0:T(8,128)}, u32[]{:S(2)}) copy-start(f32[4,768,512,2]{2,1,3,0:T(8,128)} %get-tuple-element.199) | copy-start | bytes 37748740 | tf_op jit(solution)/shard_map/while
  61.8 9.0 %copy-start.2 = (bf16[1,768,256]{1,2,0:T(8,128)(2,1)S(1)}, bf16[1,768,256]{1,2,0:T(8,128)(2,1)}, u32[]{:S(2)}) copy-start(bf16[1,768,256]{1,2,0:T(8,128)(2,1)} %get-tuple-element.195) | copy-start | bytes 1179652 | tf_op jit(solution)/shard_map/while
  131.8 1.2 copy-start.4
  133.0 0.8 copy-start.5
  133.0 0.8 copy-start.6
  136.9 74.5 %all-to-all-start.1 = ((bf16[4,256,2048]{2,1,0:T(8,128)(2,1)}), bf16[4,256,2048]{2,1,0:T(8,128)(2,1)}, u32[]{:S(2)}, u32[]{:S(2)}) async-start(bf16[4,256,2048]{2,1,0:T(8,128)(2,1)} %broadcast_in_dim.27), calls=%async_computation.1 | async-start | bytes 8388608 | tf_op jit(solution)/shard_map/all_to_all | solution.py:53
  141.7 147.1 %reduce-scatter.2.cloned.1.call-start = ((), (), s32[]{:S(2)}) async-start(), calls=%async_computation.3 | async-start | bytes 5242880 | tf_op jit(solution)/shard_map/reduce_scatter | solution.py:145
  237.0 55.2 %copy-start.7 = (f32[2048]{0:T(1024)S(1)}, f32[2048]{0:T(1024)}, u32[]{:S(2)}) copy-start(f32[2048]{0:T(1024)} %param.23) | copy-start | bytes 24580
  237.0 55.2 %copy-start.8 = (f32[2048]{0:T(1024)S(1)}, f32[2048]{0:T(1024)}, u32[]{:S(2)}) copy-start(f32[2048]{0:T(1024)} %param.22) | copy-start | bytes 24580
  288.8 3.4 %copy-start.3 = (bf16[256,2048]{1,0:T(8,128)(2,1)S(1)}, bf16[256,2048]{1,0:T(8,128)(2,1)}, u32[]{:S(2)}) copy-start(bf16[256,2048]{1,0:T(8,128)(2,1)} %reduce-scatter.2.cloned.1.call-done) | copy-start | bytes 3145732
Sparse Core Ops, SparseCore 0:
  10.2 76.2 all-gather.2
  237.1 51.6 reduce-scatter.1
where the time goes:
time: 302 us; the launch traced here: 301 us
  local copies, waits for them, and re-layouts  90.2 us (30%)
  waiting for transfers between devices  53.6 us (18%)
  blocking collectives  52.5 us (17%)
  matrix products  51.9 us (17%)
  other arithmetic  26.1 us (9%)
  between operations  13.6 us (5%)
  starting transfers between devices  11.4 us (4%)
    all_to_all x1, blocking collectives, sent_and_summed(): lax.all_to_all(pieces, axis, split_axis=0, concat_axis=0, tiled=True)  52.5 us
    reduce_scatter x1, waiting for transfers between devices, on_device(): lax.psum_scatter(jnp.dot(rows, down_full, preferred_element_type=jnp.floa...  51.8 us
    dot_general x1, matrix products, on_device(): jnp.dot(rows, down_full, preferred_element_type=jnp.float32)  25.7 us
    reshape x1, local copies, waits for them, and re-layouts, one_gather(): pieces = lines[:, at:at + a.size].reshape(-1, *a.shape)  19 us
    transpose x1, local copies, waits for them, and re-layouts, in_order(): return jnp.moveaxis(pieces, 0, dim).reshape(dims)  15.8 us
    dot_general x2, matrix products, one_block(): jnp.einsum('qhgd,khd->hgqk', query, keys, preferred_element_type=jnp.floa...  15.3 us
    reduce_sum x2, other arithmetic, one_block(): denom = jnp.sum(expd, axis=-1, keepdims=True) + jnp.exp(sink - top)  15.1 us
    all_gather x1, local copies, waits for them, and re-layouts, one_gather(): lines, at, finished = (lax.all_gather(flat, axis), 0, [])  14.6 us
  transfers between devices with their start and end apart: 5, of which 3 were waited for; matrix products, arithmetic and copies ran while one was open for 44% of the time, Pallas kernels for 0%

commit v1 on v0

v1 whole, which is shorter than its diff:
```python
import functools

import jax
import jax.numpy as jnp
from jax import lax
from jax.experimental import pallas as pl
from jax.experimental.pallas import tpu as pltpu
from jax.sharding import PartitionSpec as P

HEAD_DIM = 64
WINDOW = 128
MESH = pl.DeviceIdType.MESH
N_COPIES = 104
F32 = jnp.float32
BF16 = jnp.bfloat16


def norm_rows(values, gain, bias):
    mean = jnp.mean(values, axis=-1, keepdims=True)
    centred = values - mean
    variance = jnp.mean(centred * centred, axis=-1, keepdims=True)
    return (centred * lax.rsqrt(variance + 1e-06) * gain + bias).astype(BF16)


class Plane:
    def __init__(self, send, acc, z, y):
        self.send, self.acc, self.z, self.y = send, acc, z, y
        self.zs = (lax.rem(z + 1, 4), lax.rem(z + 3, 4), lax.rem(z + 2, 4))
        self.ys = (lax.rem(y + 1, 4), lax.rem(y + 3, 4), lax.rem(y + 2, 4))
        self.cross = []

    def own_piece(self):
        acc, z, y = self.acc, self.z, self.y
        a, b = acc(z, y, 0, None), acc(z, y, 1, None)
        self.near = [self.send(a, "y+"), self.send(a, "y-"), self.send(b, "z+"), self.send(b, "z-")]

    def own_piece_on(self):
        acc, z, y = self.acc, self.z, self.y
        for copy in self.near:
            copy.wait_recv()
        self.far = [
            self.send(acc(z, self.ys[1], 0, 0), "y+"),
            self.send(acc(z, self.ys[0], 0, 1), "y-"),
            self.send(acc(self.zs[1], y, 1, 0), "z+"),
            self.send(acc(self.zs[0], y, 1, 1), "z-"),
        ]

    def line(self):
        acc, z, y = self.acc, self.z, self.y
        every = slice(None)
        for copy in self.far:
            copy.wait_recv()
        self.first = [
            self.send(acc(z, every, 0, 0), "z+"),
            self.send(acc(z, every, 0, 1), "z-"),
            self.send(acc(every, y, 1, 0), "y+"),
            self.send(acc(every, y, 1, 1), "y-"),
        ]
        self.second = [
            self.send(acc(z, every, 0, 1), "z+"),
            self.send(acc(z, every, 0, 0), "z-"),
            self.send(acc(every, y, 1, 1), "y+"),
            self.send(acc(every, y, 1, 0), "y-"),
        ]
        self.to_partner(z, y)

    def to_partner(self, z, y):
        every = slice(None)
        self.cross.append(self.send(self.acc(z, every, 0, None), "core"))
        self.cross.append(self.send(self.acc(every, y, 1, None), "core"))

    def line_on(self):
        acc = self.acc
        every = slice(None)
        for copy in self.first:
            copy.wait_recv()
        self.last = [
            self.send(acc(self.zs[1], every, 0, 0), "z+"),
            self.send(acc(self.zs[0], every, 0, 1), "z-"),
            self.send(acc(every, self.ys[1], 1, 0), "y+"),
            self.send(acc(every, self.ys[0], 1, 1), "y-"),
        ]

    def neighbours(self):
        for copy in self.second:
            copy.wait_recv()
        self.to_partner(self.zs[0], self.ys[0])
        self.to_partner(self.zs[1], self.ys[1])

    def opposite(self):
        for copy in self.last:
            copy.wait_recv()
        self.to_partner(self.zs[2], self.ys[2])

    def finish(self):
        for copy in self.cross:
            copy.wait_recv()


def layer_kernel(
    total,
    res_hbm,
    q_hbm,
    kv_hbm,
    sink_ref,
    ow_hbm,
    g1_ref,
    b1_ref,
    up_hbm,
    dn_hbm,
    g2_ref,
    b2_ref,
    out_ref,
    q_ref,
    kv_ref,
    res_ref,
    bias_ref,
    att_ref,
    afull_ref,
    wo_ref,
    wu_ref,
    wd_ref,
    pre_ref,
    tok_ref,
    act_ref,
    part_ref,
    rin_ref,
    fin_ref,
    loc_sem,
    send_sem,
    recv_sem,
):
    sp = lax.axis_index("sp")
    x = lax.axis_index("tp")
    z, y, c = sp // 8, lax.rem(sp // 2, 4), lax.rem(sp, 2)
    right, left, opp = lax.rem(x + 1, 4), lax.rem(x + 3, 4), lax.rem(x + 2, 4)

    def at(zz, yy, cc):
        return {"sp": zz * 8 + yy * 2 + cc, "tp": x}

    where_to = {
        "y+": at(z, lax.rem(y + 1, 4), c),
        "y-": at(z, lax.rem(y + 3, 4), c),
        "z+": at(lax.rem(z + 1, 4), y, c),
        "z-": at(lax.rem(z + 3, 4), y, c),
        "core": at(z, y, 1 - c),
        "x+": {"sp": sp, "tp": right},
        "x-": {"sp": sp, "tp": left},
        "xx": {"sp": sp, "tp": opp},
        "next": {"sp": lax.rem(sp + 1, 32), "tp": x},
        "prev": {"sp": lax.rem(sp + 31, 32), "tp": x},
    }

    barrier = pltpu.get_barrier_semaphore()
    for device in where_to.values():
        pl.semaphore_signal(barrier, inc=1, device_id=device, device_id_type=MESH)

    local = [
        pltpu.make_async_copy(ow_hbm, wo_ref.at[0], loc_sem.at[0]),
        pltpu.make_async_copy(kv_hbm, kv_ref.at[:, pl.ds(WINDOW, 1024)], loc_sem.at[1]),
        pltpu.make_async_copy(up_hbm, wu_ref.at[z, y, c], loc_sem.at[2]),
        pltpu.make_async_copy(dn_hbm, wd_ref.at[z, y, c], loc_sem.at[3]),
        pltpu.make_async_copy(q_hbm, q_ref, loc_sem.at[4]),
        pltpu.make_async_copy(res_hbm, res_ref, loc_sem.at[5]),
    ]
    for copy in local:
        copy.start()
    started = []

    def send_to(src, dst, where):
        k = len(started)
        copy = pltpu.make_async_remote_copy(
            src_ref=src,
            dst_ref=dst,
            send_sem=send_sem.at[k],
            recv_sem=recv_sem.at[k],
            device_id=where_to[where],
            device_id_type=MESH,
        )
        copy.start()
        started.append(copy)
        return copy

    def send_same(ref, where):
        return send_to(ref, ref, where)

    def rows_of(ref):
        def acc(zz, yy, half, sub):
            low = half * 32 + (sub or 0) * 16
            return ref.at[zz, yy, c, pl.ds(low, 32 if sub is None else 16)]

        return acc

    def cols_of(zz, yy, half, sub):
        low = half * 1024 + (sub or 0) * 512
        return wo_ref.at[pl.ds(1, 3), zz, yy, c, :, pl.ds(low, 1024 if sub is None else 512)]

    out_w = Plane(send_same, cols_of, z, y)
    up_w = Plane(send_same, rows_of(wu_ref), z, y)
    dn_w = Plane(send_same, rows_of(wd_ref), z, y)

    pl.semaphore_wait(barrier, len(where_to))
    local[0].wait()
    mine = wo_ref.at[0, z, y, c]
    exchange = [
        send_to(mine, wo_ref.at[3, z, y, c], "x+"),
        send_to(mine, wo_ref.at[1, z, y, c], "x-"),
        send_to(mine, wo_ref.at[2, z, y, c], "xx"),
    ]
    local[1].wait()
    halo = [
        send_to(kv_ref.at[:, pl.ds(1024, 128)], kv_ref.at[:, pl.ds(0, 128)], "next"),
        send_to(kv_ref.at[:, pl.ds(128, 128)], kv_ref.at[:, pl.ds(1152, 128)], "prev"),
    ]
    local[2].wait()
    up_w.own_piece()
    local[3].wait()
    dn_w.own_piece()
    local[4].wait()
    for copy in halo:
        copy.wait_recv()

    low_lanes = lax.broadcasted_iota(jnp.int32, (128, 128), 1) < 64
    low_keys = lax.broadcasted_iota(jnp.int32, (384, 128), 1) < 64
    first_head = lax.broadcasted_iota(jnp.int32, (256, 1), 0) < 128

    def attend_block(start, dst_ref, dst_row):
        row = lax.broadcasted_iota(jnp.int32, (128, 384), 0)
        col = lax.broadcasted_iota(jnp.int32, (128, 384), 1)
        key_pos = sp * 1024 + start - WINDOW + col
        valid = (col >= row) & (col <= row + 2 * WINDOW) & (key_pos >= 0) & (key_pos < total)
        bias_ref[...] = jnp.where(valid, 0.0, -1e30)
        for g in range(4):
            query = q_ref[pl.ds(start, 128), g * 128 : (g + 1) * 128].astype(F32) * 0.125
            swapped = pltpu.roll(query, 64, 1)
            lanes = slice((g // 2) * 128, (g // 2) * 128 + 128)
            keys = kv_ref[0, pl.ds(start, 384), lanes]
            values = kv_ref[1, pl.ds(start, 384), lanes]
            ones = jnp.ones_like(values)
            if g % 2 == 0:
                stacked = [jnp.where(low_lanes, query, 0.0), jnp.where(low_lanes, swapped, 0.0)]
                values = jnp.where(low_keys, values, ones)
            else:
                stacked = [jnp.where(low_lanes, 0.0, swapped), jnp.where(low_lanes, 0.0, query)]
                values = jnp.where(low_keys, ones, values)
            stacked = jnp.concatenate(stacked, axis=0).astype(BF16)
            scores = lax.dot_general(
                stacked, keys, (((1,), (1,)), ((), ())), preferred_element_type=F32
            )
            bias = bias_ref[...]
            scores = scores + jnp.concatenate([bias, bias], axis=0)
            sink = jnp.where(first_head, sink_ref[2 * g], sink_ref[2 * g + 1])
            top = jnp.maximum(jnp.max(scores, axis=1, keepdims=True), sink)
            weights = jnp.exp(scores - top).astype(BF16)
            rest = jnp.exp(sink - top)
            mixed = jnp.dot(weights, values, preferred_element_type=F32)
            a, b = mixed[:128], mixed[128:]
            a_swapped, b_swapped = pltpu.roll(a, 64, 1), pltpu.roll(b, 64, 1)
            if g % 2 == 0:
                num = jnp.where(low_lanes, a, b_swapped)
                den = jnp.where(low_lanes, a_swapped, b)
            else:
                num = jnp.where(low_lanes, a_swapped, b)
                den = jnp.where(low_lanes, a, b_swapped)
            den = den + jnp.where(low_lanes, rest[:128], rest[128:])
            dst_ref[pl.ds(dst_row, 128), g * 128 : (g + 1) * 128] = (num / den).astype(BF16)

    def attend_quarter(owner, dst_ref):
        @pl.loop(0, 2)
        def _(i):
            row = pl.multiple_of(i * 128, 128)
            attend_block(pl.multiple_of(owner * 256 + row, 128), dst_ref, row)

    mixes = []
    attend_quarter(opp, att_ref.at[0])
    mixes.append(send_to(att_ref.at[0], afull_ref.at[:, pl.ds(1024, 512)], "xx"))
    for copy in exchange:
        copy.wait_recv()
    out_w.own_piece()
    attend_quarter(right, att_ref.at[1])
    mixes.append(send_to(att_ref.at[1], afull_ref.at[:, pl.ds(1536, 512)], "x+"))
    out_w.own_piece_on()
    up_w.own_piece_on()
    dn_w.own_piece_on()
    attend_quarter(left, att_ref.at[2])
    mixes.append(send_to(att_ref.at[2], afull_ref.at[:, pl.ds(512, 512)], "x-"))
    out_w.line()
    attend_quarter(x, afull_ref.at[:, pl.ds(0, 512)])
    out_w.line_on()
    up_w.line()
    out_w.neighbours()
    out_w.opposite()
    local[5].wait()
    for copy in mixes:
        copy.wait_recv()
    out_w.finish()

    @pl.loop(0, 4)
    def _(n):
        cols = pl.ds(pl.multiple_of(n * 512, 512), 512)
        weight = wo_ref[:, :, :, :, :, cols].reshape(2048, 512)
        pre_ref[:, cols] = res_ref[:, cols].astype(F32) + jnp.dot(
            afull_ref[...], weight, preferred_element_type=F32
        )

    def first_norm(part):
        @pl.loop(0, 2)
        def _(i):
            rows = pl.ds(pl.multiple_of(part * 128 + i * 64, 64), 64)
            tok_ref[0, rows, :] = norm_rows(pre_ref[rows, :], g1_ref[...], b1_ref[...])

    top, bottom = pl.ds(0, 128), pl.ds(128, 128)
    first_norm(0)
    top_right = send_to(tok_ref.at[0, top], tok_ref.at[3, top], "x+")
    first_norm(1)
    bottom_left = send_to(tok_ref.at[0, bottom], tok_ref.at[1, bottom], "x-")
    bottom_right = send_to(tok_ref.at[0, bottom], tok_ref.at[3, bottom], "x+")
    top_left = send_to(tok_ref.at[0, top], tok_ref.at[1, top], "x-")

    up_w.line_on()
    dn_w.line()
    top_right.wait_recv()
    top_on = send_to(tok_ref.at[3, top], tok_ref.at[2, top], "x+")
    bottom_left.wait_recv()
    bottom_on = send_to(tok_ref.at[1, bottom], tok_ref.at[2, bottom], "x-")
    up_w.neighbours()
    up_w.opposite()
    dn_w.line_on()
    dn_w.neighbours()
    dn_w.opposite()
    up_w.finish()
    dn_w.finish()

    def feed_forward(slot, dst_ref):
        @pl.loop(0, 4)
        def _(n):
            cols = pl.ds(pl.multiple_of(n * 512, 512), 512)
            weight = wu_ref[:, :, :, :, cols].reshape(2048, 512)
            hidden = jnp.dot(tok_ref[slot], weight, preferred_element_type=F32)
            act_ref[:, cols] = jnp.square(jnp.maximum(hidden, 0.0)).astype(BF16)

        @pl.loop(0, 4)
        def _(n):
            cols = pl.ds(pl.multiple_of(n * 512, 512), 512)
            weight = wd_ref[n].reshape(512, 2048)
            dst_ref[:, cols] = lax.dot_general(
                act_ref[...], weight, (((1,), (1,)), ((), ())), preferred_element_type=F32
            ).astype(dst_ref.dtype)

    feed_forward(0, pre_ref)
    bottom_right.wait_recv()
    feed_forward(3, part_ref.at[0])
    sums = [send_to(part_ref.at[0, top], fin_ref.at[1, top], "x-")]
    top_left.wait_recv()
    feed_forward(1, part_ref.at[1])
    sums.append(send_to(part_ref.at[1, bottom], fin_ref.at[0, bottom], "x+"))
    top_on.wait_recv()
    bottom_on.wait_recv()
    feed_forward(2, part_ref.at[2])
    far = [
        send_to(part_ref.at[2, top], rin_ref.at[0], "x+"),
        send_to(part_ref.at[2, bottom], rin_ref.at[1], "x-"),
    ]
    far[0].wait_recv()
    part_ref[1, top, :] = (part_ref[1, top, :].astype(F32) + rin_ref[0].astype(F32)).astype(BF16)
    sums.append(send_to(part_ref.at[1, top], fin_ref.at[0, top], "x+"))
    far[1].wait_recv()
    part_ref[0, bottom, :] = (part_ref[0, bottom, :].astype(F32) + rin_ref[1].astype(F32)).astype(BF16)
    sums.append(send_to(part_ref.at[0, bottom], fin_ref.at[1, bottom], "x-"))
    for copy in sums:
        copy.wait_recv()

    @pl.loop(0, 4)
    def _(i):
        rows = pl.ds(pl.multiple_of(i * 64, 64), 64)
        branch = pre_ref[rows, :] + fin_ref[0, rows, :].astype(F32) + fin_ref[1, rows, :].astype(F32)
        out_ref[rows, :] = norm_rows(
            tok_ref[0, rows, :].astype(F32) + branch, g2_ref[...], b2_ref[...]
        )

    for copy in started:
        copy.wait_send()


def on_device(
    residual_in,
    queries,
    keys_values,
    sink_logit,
    out_weight,
    norm1_gain,
    norm1_bias,
    up_weight,
    down_weight,
    norm2_gain,
    norm2_bias,
):
    total = queries.shape[0] * lax.axis_size("sp")
    any_spec = pl.BlockSpec(memory_space=pl.ANY)
    vmem = pl.BlockSpec(memory_space=pltpu.VMEM)
    smem = pl.BlockSpec(memory_space=pltpu.SMEM)
    row = lambda v: v.reshape(1, -1)
    return pl.pallas_call(
        functools.partial(layer_kernel, total),
        out_shape=jax.ShapeDtypeStruct(residual_in.shape, BF16),
        in_specs=[any_spec, any_spec, any_spec, smem, any_spec, vmem, vmem, any_spec, any_spec, vmem, vmem],
        out_specs=vmem,
        scratch_shapes=[
            pltpu.VMEM((1024, 512), BF16),
            pltpu.VMEM((2, 1280, 256), BF16),
            pltpu.VMEM((256, 2048), BF16),
            pltpu.VMEM((128, 384), F32),
            pltpu.VMEM((3, 256, 512), BF16),
            pltpu.VMEM((256, 2048), BF16),
            pltpu.VMEM((4, 4, 4, 2, 16, 2048), BF16),
            pltpu.VMEM((4, 4, 2, 64, 2048), BF16),
            pltpu.VMEM((4, 4, 2, 64, 2048), BF16),
            pltpu.VMEM((256, 2048), F32),
            pltpu.VMEM((4, 256, 2048), BF16),
            pltpu.VMEM((256, 2048), BF16),
            pltpu.VMEM((3, 256, 2048), BF16),
            pltpu.VMEM((2, 128, 2048), BF16),
            pltpu.VMEM((2, 256, 2048), BF16),
            pltpu.SemaphoreType.DMA((6,)),
            pltpu.SemaphoreType.DMA((N_COPIES,)),
            pltpu.SemaphoreType.DMA((N_COPIES,)),
        ],
        compiler_params=pltpu.CompilerParams(
            collective_id=0, has_side_effects=True, vmem_limit_bytes=67000000
        ),
        name="layer",
    )(
        residual_in,
        queries,
        keys_values,
        sink_logit,
        out_weight.reshape(4, 4, 2, 16, 2048),
        row(norm1_gain),
        row(norm1_bias),
        up_weight,
        down_weight.T,
        row(norm2_gain),
        row(norm2_bias),
    )


def solution(mesh):
    return jax.shard_map(
        on_device,
        mesh=mesh,
        in_specs=(
            P(("sp", "tp"), None),
            P("sp", "tp"),
            P(None, "sp", "tp"),
            P("tp"),
            P("tp", None),
            P(),
            P(),
            P("sp", "tp"),
            P("tp", "sp"),
            P(),
            P(),
        ),
        out_specs=P(("sp", "tp"), None),
        check_vma=False,
    )
```

time: 302 us -> 138 us (0.46)
  Pallas kernels: 0 us -> 135 us
  local copies, waits for them, and re-layouts: 90.2 us -> 2.3 us
  waiting for transfers between devices: 53.6 us -> 0 us
  blocking collectives: 52.5 us -> 0 us
  matrix products: 51.9 us -> 0 us
  other arithmetic: 26.1 us -> 0 us
  between operations: 13.6 us -> 0.01 us
  starting transfers between devices: 11.4 us -> 0 us
    pallas_call x0 -> x1, Pallas kernels: none -> 135 us  [on_device(): pl.pallas_call(functools.partial(layer_kernel, total), out_shape=jax.Shap...]
    all_to_all x1 -> x0, blocking collectives: 52.5 us -> none  [sent_and_summed(): lax.all_to_all(pieces, axis, split_axis=0, concat_axis=0, tiled=True)]
    dot_general x6 -> x0, matrix products: 51.9 us -> none  [the longest x1 25.7 us: on_device(): jnp.dot(rows, down_full, preferred_element_type=jnp.float32)]
    reduce_scatter x1 -> x0, waiting for transfers between devices: 51.8 us -> none  [on_device(): lax.psum_scatter(jnp.dot(rows, down_full, preferred_element_type=jnp.floa...]
    reduce_sum x7 -> x0, other arithmetic: 20.1 us -> none  [the longest x2 15.1 us: one_block(): denom = jnp.sum(expd, axis=-1, keepdims=True) + jnp.exp(sink - top)]
    reshape x3 -> x0, local copies, waits for them, and re-layouts: 19.3 us -> none  [the longest x1 19 us: one_gather(): pieces = lines[:, at:at + a.size].reshape(-1, *a.shape)]
    transpose x1 -> x0, local copies, waits for them, and re-layouts: 15.8 us -> none  [in_order(): return jnp.moveaxis(pieces, 0, dim).reshape(dims)]
    slice x4 -> x0, local copies, waits for them, and re-layouts: 14.8 us -> none  [the longest x1 11.3 us: one_gather(): pieces = lines[:, at:at + a.size].reshape(-1, *a.shape)]
  transfers between devices with their start and end apart: 5 -> 0, of which waited for: 3 -> 0; matrix products, arithmetic and copies ran while one was open for 44% -> 0% of each run, Pallas kernels for 0% -> 0%
where the time goes in v1:
time: 138 us; the launch traced here: 137 us
  Pallas kernels  135 us (98%)
  local copies, waits for them, and re-layouts  2.3 us (2%)
    pallas_call x1, Pallas kernels, on_device(): pl.pallas_call(functools.partial(layer_kernel, total), out_shape=jax.Shap...  135 us

profile of v1, /device:TPU:1, one launch (start us, length us, event | category | flops | bytes accessed | tf_op | source)
XLA Modules:
  0.0 137.5 jit_solution(23919032455568054)
XLA Ops:
  0.0 135.2 %layer.1 = bf16[256,2048]{1,0:T(8,128)(2,1)} custom-call(bf16[256,2048]{1,0:T(8,128)(2,1)} %res_hbm.1, bf16[1024,512]{1,0:T(8,128)(2,1)} %q_hbm.1, bf16[2,1024,256]{2,1,0:T(8,128)(2,1)} %kv_hbm.1, f32[8]{0:T(128)} %sink_ref.1, bf16[4,4,2,16,2048]{4,3,2,1,0:T(8,128)(2,1)} %bitcast.6, f32[1,2048]{1,0:T(1,128)} %bitcast.8, f32[1,2048]{1,0:T(1,128)} %bitcast.9, ...), custom_call_target="tpu_custom_call" | custom-call | tf_op jit(solution)/shard_map/layer/pallas_call | solution.py:403
  135.2 2.3 %copy.13 = bf16[256,2048]{1,0:T(8,128)(2,1)} copy(bf16[256,2048]{1,0:T(8,128)(2,1)} %layer.1) | data formatting | bytes 2097152

commit v2 on v1

--- a/solution.py
+++ b/solution.py
@@ -10,7 +10,7 @@
 HEAD_DIM = 64
 WINDOW = 128
 MESH = pl.DeviceIdType.MESH
-N_COPIES = 104
+N_COPIES = 143
 F32 = jnp.float32
 BF16 = jnp.bfloat16
 
@@ -95,6 +95,53 @@
     def finish(self):
         for copy in self.cross:
             copy.wait_recv()
+
+
+class Waves(Plane):
+    def both_ways(self, yz):
+        acc = self.acc
+        (ya, za), (yb, zb) = yz
+        return [
+            self.send(acc(za, ya, 0, None), "z+"),
+            self.send(acc(za, ya, 0, None), "z-"),
+            self.send(acc(zb, yb, 1, None), "y+"),
+            self.send(acc(zb, yb, 1, None), "y-"),
+        ]
+
+    def onward(self, copies, yy, zz):
+        acc = self.acc
+        for copy in copies:
+            copy.wait_recv()
+        return [
+            self.send(acc(self.zs[1], yy, 0, 0), "z+"),
+            self.send(acc(self.zs[0], yy, 0, 1), "z-"),
+            self.send(acc(zz, self.ys[1], 1, 0), "y+"),
+            self.send(acc(zz, self.ys[0], 1, 1), "y-"),
+        ]
+
+    def start(self):
+        self.own_piece()
+        self.wave0 = self.both_ways(((self.y, self.z), (self.y, self.z)))
+
+    def step1(self):
+        self.own_piece_on()
+        self.waves1 = []
+        for i in (0, 1):
+            self.waves1.append(self.both_ways(((self.ys[i], self.z), (self.y, self.zs[i]))))
+        self.last = self.onward(self.wave0, self.y, self.z)
+
+    def step2(self):
+        for copy in self.far:
+            copy.wait_recv()
+        self.wave2 = self.both_ways(((self.ys[2], self.z), (self.y, self.zs[2])))
+        for i in (0, 1):
+            self.last += self.onward(self.waves1[i], self.ys[i], self.zs[i])
+
+    def step3(self):
+        self.last += self.onward(self.wave2, self.ys[2], self.zs[2])
+        self.to_partner(self.z, self.y)
+        self.to_partner(self.zs[0], self.ys[0])
+        self.to_partner(self.zs[1], self.ys[1])
 
 
 def layer_kernel(
@@ -192,20 +239,30 @@
         return acc
 
     def cols_of(zz, yy, half, sub):
-        low = half * 1024 + (sub or 0) * 512
-        return wo_ref.at[pl.ds(1, 3), zz, yy, c, :, pl.ds(low, 1024 if sub is None else 512)]
-
-    out_w = Plane(send_same, cols_of, z, y)
+        low = half * 768 + (sub or 0) * 384
+        return wo_ref.at[pl.ds(1, 3), zz, yy, c, :, pl.ds(low, 768 if sub is None else 384)]
+
+    def tail(slot, zz, depth):
+        return wo_ref.at[slot, pl.ds(zz, depth), :, :, :, pl.ds(1536, 512)]
+
+    out_w = Waves(send_same, cols_of, z, y)
     up_w = Plane(send_same, rows_of(wu_ref), z, y)
     dn_w = Plane(send_same, rows_of(wd_ref), z, y)
 
     pl.semaphore_wait(barrier, len(where_to))
     local[0].wait()
-    mine = wo_ref.at[0, z, y, c]
+    spread = pl.ds(0, 1536)
+    mine = wo_ref.at[0, z, y, c, :, spread]
     exchange = [
-        send_to(mine, wo_ref.at[3, z, y, c], "x+"),
-        send_to(mine, wo_ref.at[1, z, y, c], "x-"),
-        send_to(mine, wo_ref.at[2, z, y, c], "xx"),
+        send_to(mine, wo_ref.at[3, z, y, c, :, spread], "x+"),
+        send_to(mine, wo_ref.at[1, z, y, c, :, spread], "x-"),
+        send_to(mine, wo_ref.at[2, z, y, c, :, spread], "xx"),
+    ]
+    tails = [
+        send_to(tail(0, 2 * c, 1), tail(3, 2 * c, 1), "x+"),
+        send_to(tail(0, 2 * c + 1, 1), tail(1, 2 * c + 1, 1), "x-"),
+        send_to(tail(0, 2 * c + 1, 1), tail(3, 2 * c + 1, 1), "x+"),
+        send_to(tail(0, 2 * c, 1), tail(1, 2 * c, 1), "x-"),
     ]
     local[1].wait()
     halo = [
@@ -216,6 +273,9 @@
     up_w.own_piece()
     local[3].wait()
     dn_w.own_piece()
+    for copy in exchange:
+        copy.wait_recv()
+    out_w.start()
     local[4].wait()
     for copy in halo:
         copy.wait_recv()
@@ -274,33 +334,57 @@
     mixes = []
     attend_quarter(opp, att_ref.at[0])
     mixes.append(send_to(att_ref.at[0], afull_ref.at[:, pl.ds(1024, 512)], "xx"))
-    for copy in exchange:
-        copy.wait_recv()
-    out_w.own_piece()
     attend_quarter(right, att_ref.at[1])
     mixes.append(send_to(att_ref.at[1], afull_ref.at[:, pl.ds(1536, 512)], "x+"))
-    out_w.own_piece_on()
-    up_w.own_piece_on()
-    dn_w.own_piece_on()
+    out_w.step1()
+    for copy in tails[:2]:
+        copy.wait_recv()
+    tails_on = [
+        send_to(tail(3, 2 * c, 1), tail(2, 2 * c, 1), "x+"),
+        send_to(tail(1, 2 * c + 1, 1), tail(2, 2 * c + 1, 1), "x-"),
+    ]
     attend_quarter(left, att_ref.at[2])
     mixes.append(send_to(att_ref.at[2], afull_ref.at[:, pl.ds(512, 512)], "x-"))
-    out_w.line()
+    out_w.step2()
+    for copy in tails[2:]:
+        copy.wait_recv()
+    tails += [
+        send_same(tail(3, 2 * c, 2), "core"),
+        send_same(tail(1, 2 * c, 2), "core"),
+    ]
     attend_quarter(x, afull_ref.at[:, pl.ds(0, 512)])
-    out_w.line_on()
-    up_w.line()
-    out_w.neighbours()
-    out_w.opposite()
+    out_w.step3()
+    up_w.own_piece_on()
     local[5].wait()
-    for copy in mixes:
-        copy.wait_recv()
-    out_w.finish()
 
     @pl.loop(0, 4)
     def _(n):
         cols = pl.ds(pl.multiple_of(n * 512, 512), 512)
-        weight = wo_ref[:, :, :, :, :, cols].reshape(2048, 512)
         pre_ref[:, cols] = res_ref[:, cols].astype(F32) + jnp.dot(
-            afull_ref[...], weight, preferred_element_type=F32
+            afull_ref[:, 0:512],
+            wo_ref[0, :, :, :, :, cols].reshape(512, 512),
+            preferred_element_type=F32,
+        )
+
+    for copy in tails_on:
+        copy.wait_recv()
+    tails.append(send_same(tail(2, 2 * c, 2), "core"))
+    out_w.opposite()
+    dn_w.own_piece_on()
+    up_w.line()
+    for copy in mixes:
+        copy.wait_recv()
+    out_w.finish()
+    for copy in tails[4:]:
+        copy.wait_recv()
+
+    @pl.loop(0, 4)
+    def _(n):
+        cols = pl.ds(pl.multiple_of(n * 512, 512), 512)
+        pre_ref[:, cols] += jnp.dot(
+            afull_ref[:, 512:2048],
+            wo_ref[1:4, :, :, :, :, cols].reshape(1536, 512),
+            preferred_element_type=F32,
         )
 
     def first_norm(part):
@@ -316,6 +400,26 @@
     bottom_left = send_to(tok_ref.at[0, bottom], tok_ref.at[1, bottom], "x-")
     bottom_right = send_to(tok_ref.at[0, bottom], tok_ref.at[3, bottom], "x+")
     top_left = send_to(tok_ref.at[0, top], tok_ref.at[1, top], "x-")
+
+    def up_project(block, get_rows):
+        @pl.loop(0, 4)
+        def _(n):
+            cols = pl.ds(pl.multiple_of(n * 512, 512), 512)
+            weight = wu_ref[:, :, :, :, cols].reshape(2048, 512)
+            hidden = jnp.dot(get_rows(), weight, preferred_element_type=F32)
+            act_ref[block, :, cols] = jnp.square(jnp.maximum(hidden, 0.0)).astype(BF16)
+
+    def down_project(block, dst_ref):
+        @pl.loop(0, 4)
+        def _(n):
+            cols = pl.ds(pl.multiple_of(n * 512, 512), 512)
+            weight = wd_ref[n].reshape(512, 2048)
+            dst_ref[:, cols] = lax.dot_general(
+                act_ref[block], weight, (((1,), (1,)), ((), ())), preferred_element_type=F32
+            ).astype(dst_ref.dtype)
+
+    def two_halves(left_rows, right_rows):
+        return lambda: jnp.concatenate([tok_ref[3, left_rows, :], tok_ref[1, right_rows, :]], axis=0)
 
     up_w.line_on()
     dn_w.line()
@@ -325,59 +429,64 @@
     bottom_on = send_to(tok_ref.at[1, bottom], tok_ref.at[2, bottom], "x-")
     up_w.neighbours()
     up_w.opposite()
+    up_w.finish()
+    up_project(0, two_halves(top, bottom))
     dn_w.line_on()
+    up_project(3, lambda: tok_ref[0])
     dn_w.neighbours()
+    bottom_right.wait_recv()
+    top_left.wait_recv()
+    up_project(2, two_halves(bottom, top))
     dn_w.opposite()
-    up_w.finish()
     dn_w.finish()
-
-    def feed_forward(slot, dst_ref):
-        @pl.loop(0, 4)
-        def _(n):
-            cols = pl.ds(pl.multiple_of(n * 512, 512), 512)
-            weight = wu_ref[:, :, :, :, cols].reshape(2048, 512)
-            hidden = jnp.dot(tok_ref[slot], weight, preferred_element_type=F32)
-            act_ref[:, cols] = jnp.square(jnp.maximum(hidden, 0.0)).astype(BF16)
-
-        @pl.loop(0, 4)
-        def _(n):
-            cols = pl.ds(pl.multiple_of(n * 512, 512), 512)
-            weight = wd_ref[n].reshape(512, 2048)
-            dst_ref[:, cols] = lax.dot_general(
-                act_ref[...], weight, (((1,), (1,)), ((), ())), preferred_element_type=F32
-            ).astype(dst_ref.dtype)
-
-    feed_forward(0, pre_ref)
-    bottom_right.wait_recv()
-    feed_forward(3, part_ref.at[0])
-    sums = [send_to(part_ref.at[0, top], fin_ref.at[1, top], "x-")]
-    top_left.wait_recv()
-    feed_forward(1, part_ref.at[1])
-    sums.append(send_to(part_ref.at[1, bottom], fin_ref.at[0, bottom], "x+"))
+    pure = []
+    for n in range(4):
+        cols = pl.ds(n * 512, 512)
+        part_ref[0, :, cols] = lax.dot_general(
+            act_ref[0],
+            wd_ref[n].reshape(512, 2048),
+            (((1,), (1,)), ((), ())),
+            preferred_element_type=F32,
+        ).astype(BF16)
+        pure.append(send_to(part_ref.at[0, top, cols], fin_ref.at[1, top, cols], "x-"))
+        pure.append(send_to(part_ref.at[0, bottom, cols], fin_ref.at[0, bottom, cols], "x+"))
     top_on.wait_recv()
     bottom_on.wait_recv()
-    feed_forward(2, part_ref.at[2])
-    far = [
-        send_to(part_ref.at[2, top], rin_ref.at[0], "x+"),
-        send_to(part_ref.at[2, bottom], rin_ref.at[1], "x-"),
-    ]
-    far[0].wait_recv()
-    part_ref[1, top, :] = (part_ref[1, top, :].astype(F32) + rin_ref[0].astype(F32)).astype(BF16)
-    sums.append(send_to(part_ref.at[1, top], fin_ref.at[0, top], "x+"))
-    far[1].wait_recv()
-    part_ref[0, bottom, :] = (part_ref[0, bottom, :].astype(F32) + rin_ref[1].astype(F32)).astype(BF16)
-    sums.append(send_to(part_ref.at[0, bottom], fin_ref.at[1, bottom], "x-"))
-    for copy in sums:
-        copy.wait_recv()
-
-    @pl.loop(0, 4)
-    def _(i):
-        rows = pl.ds(pl.multiple_of(i * 64, 64), 64)
+    up_project(1, lambda: tok_ref[2])
+    down_project(1, part_ref.at[2])
+    far_right, far_left = [], []
+    for i in range(2):
+        upper, lower = pl.ds(i * 64, 64), pl.ds(128 + i * 64, 64)
+        far_right.append(send_to(part_ref.at[2, upper], rin_ref.at[1, upper], "x+"))
+        far_left.append(send_to(part_ref.at[2, lower], rin_ref.at[0, upper], "x-"))
+    down_project(2, part_ref.at[1])
+    down_project(3, pre_ref)
+    sum_right, sum_left = [], []
+    for i in range(2):
+        upper, lower = pl.ds(i * 64, 64), pl.ds(128 + i * 64, 64)
+        far_right[i].wait_recv()
+        part_ref[1, lower, :] = (
+            part_ref[1, lower, :].astype(F32) + rin_ref[1, upper, :].astype(F32)
+        ).astype(BF16)
+        sum_right.append(send_to(part_ref.at[1, lower], fin_ref.at[0, upper], "x+"))
+        far_left[i].wait_recv()
+        part_ref[1, upper, :] = (
+            part_ref[1, upper, :].astype(F32) + rin_ref[0, upper, :].astype(F32)
+        ).astype(BF16)
+        sum_left.append(send_to(part_ref.at[1, upper], fin_ref.at[1, lower], "x-"))
+
+    def finish_rows(low):
+        rows = pl.ds(low, 64)
         branch = pre_ref[rows, :] + fin_ref[0, rows, :].astype(F32) + fin_ref[1, rows, :].astype(F32)
-        out_ref[rows, :] = norm_rows(
-            tok_ref[0, rows, :].astype(F32) + branch, g2_ref[...], b2_ref[...]
-        )
-
+        out_ref[rows, :] = norm_rows(tok_ref[0, rows, :].astype(F32) + branch, g2_ref[...], b2_ref[...])
+
+    for copy in pure:
+        copy.wait_recv()
+    for i in range(2):
+        sum_right[i].wait_recv()
+        finish_rows(i * 64)
+        sum_left[i].wait_recv()
+        finish_rows(128 + i * 64)
     for copy in started:
         copy.wait_send()
 
@@ -402,7 +511,7 @@
     row = lambda v: v.reshape(1, -1)
     return pl.pallas_call(
         functools.partial(layer_kernel, total),
-        out_shape=jax.ShapeDtypeStruct(residual_in.shape, BF16),
+        out_shape=pltpu.VMEM(residual_in.shape, BF16),
         in_specs=[any_spec, any_spec, any_spec, smem, any_spec, vmem, vmem, any_spec, any_spec, vmem, vmem],
         out_specs=vmem,
         scratch_shapes=[
@@ -417,7 +526,7 @@
             pltpu.VMEM((4, 4, 2, 64, 2048), BF16),
             pltpu.VMEM((256, 2048), F32),
             pltpu.VMEM((4, 256, 2048), BF16),
-            pltpu.VMEM((256, 2048), BF16),
+            pltpu.VMEM((4, 256, 2048), BF16),
             pltpu.VMEM((3, 256, 2048), BF16),
             pltpu.VMEM((2, 128, 2048), BF16),
             pltpu.VMEM((2, 256, 2048), BF16),
@@ -426,7 +535,7 @@
             pltpu.SemaphoreType.DMA((N_COPIES,)),
         ],
         compiler_params=pltpu.CompilerParams(
-            collective_id=0, has_side_effects=True, vmem_limit_bytes=67000000
+            collective_id=0, has_side_effects=True, vmem_limit_bytes=58 * 1024 * 1024
         ),
         name="layer",
     )(

time: 138 us -> 115 us (0.83)
  Pallas kernels: 135 us -> 114 us
    pallas_call x1, Pallas kernels: 135 us -> 114 us  [on_device(): pl.pallas_call(functools.partial(layer_kernel, total), out_shape=pltpu.VM...]
where the time goes in v2:
time: 115 us
  Pallas kernels  114 us (99%)
    pallas_call x1, Pallas kernels, on_device(): pl.pallas_call(functools.partial(layer_kernel, total), out_shape=pltpu.VM...  114 us

profile of v2, /device:TPU:1, one launch (start us, length us, event | category | flops | bytes accessed | tf_op | source)
XLA Modules:
  0.0 114.7 jit_solution(6599676895446895187)
XLA Ops:
  0.0 113.7 %layer.1 = bf16[256,2048]{1,0:T(8,128)(2,1)S(1)} custom-call(bf16[256,2048]{1,0:T(8,128)(2,1)} %res_hbm.1, bf16[1024,512]{1,0:T(8,128)(2,1)} %q_hbm.1, bf16[2,1024,256]{2,1,0:T(8,128)(2,1)} %kv_hbm.1, f32[8]{0:T(128)} %sink_ref.1, bf16[4,4,2,16,2048]{4,3,2,1,0:T(8,128)(2,1)} %bitcast.6, f32[1,2048]{1,0:T(1,128)} %bitcast.8, f32[1,2048]{1,0:T(1,128)} %bitcast.9, ...), custom_call_target="tpu_custom_call" | custom-call | tf_op jit(solution)/shard_map/layer/pallas_call | solution.py:512
  113.7 1.0 copy.13

commit v3 on v2

v3 whole, which is shorter than its diff:
```python
import functools

import jax
import jax.numpy as jnp
from jax import lax
from jax.experimental import pallas as pl
from jax.experimental.pallas import tpu as pltpu
from jax.sharding import PartitionSpec as P

HEAD_DIM = 64
WINDOW = 128
MESH = pl.DeviceIdType.MESH
N_COPIES = 40
CHUNKS = 2
F32 = jnp.float32
BF16 = jnp.bfloat16


def norm_rows(values, gain, bias):
    mean = jnp.mean(values, axis=-1, keepdims=True)
    centred = values - mean
    variance = jnp.mean(centred * centred, axis=-1, keepdims=True)
    return (centred * lax.rsqrt(variance + 1e-06) * gain + bias).astype(BF16)


class Group:
    def __init__(self, index, link):
        self.index, self.link = index, link

    def send(self, src, dst, where):
        self.link(self.index, src, dst, where).start()

    def same(self, ref, where):
        self.send(ref, ref, where)

    def recv(self, view):
        self.whole = self.link(self.index, view, view, "x+")
        self.whole.wait_recv()

    def sent(self):
        self.whole.wait_send()


class Plane:
    def __init__(self, group, acc, z, y, views):
        self.group, self.acc, self.z, self.y = group, acc, z, y
        self.four, self.four_subs, self.four_lines, self.crossed = views
        self.zs = (lax.rem(z + 1, 4), lax.rem(z + 3, 4), lax.rem(z + 2, 4))
        self.ys = (lax.rem(y + 1, 4), lax.rem(y + 3, 4), lax.rem(y + 2, 4))
        self.cross = group()

    def quad(self, copies):
        group = self.group()
        for ref, where in copies:
            group.same(ref, where)
        return group

    def own_piece(self):
        acc, z, y = self.acc, self.z, self.y
        a, b = acc(z, y, 0, None), acc(z, y, 1, None)
        self.near = self.quad([(a, "y+"), (a, "y-"), (b, "z+"), (b, "z-")])

    def own_piece_on(self):
        acc, z, y = self.acc, self.z, self.y
        self.near.recv(self.four)
        self.far = self.quad(
            [
                (acc(z, self.ys[1], 0, 0), "y+"),
                (acc(z, self.ys[0], 0, 1), "y-"),
                (acc(self.zs[1], y, 1, 0), "z+"),
                (acc(self.zs[0], y, 1, 1), "z-"),
            ]
        )

    def line(self):
        acc, z, y = self.acc, self.z, self.y
        every = slice(None)
        self.far.recv(self.four_subs)
        self.first = self.quad(
            [
                (acc(z, every, 0, 0), "z+"),
                (acc(z, every, 0, 1), "z-"),
                (acc(every, y, 1, 0), "y+"),
                (acc(every, y, 1, 1), "y-"),
            ]
        )
        self.second = self.quad(
            [
                (acc(z, every, 0, 1), "z+"),
                (acc(z, every, 0, 0), "z-"),
                (acc(every, y, 1, 1), "y+"),
                (acc(every, y, 1, 0), "y-"),
            ]
        )
        self.to_partner(z, every, every, y)

    def to_partner(self, za, ya, zb, yb):
        self.cross.same(self.acc(za, ya, 0, None), "core")
        self.cross.same(self.acc(zb, yb, 1, None), "core")

    def line_on(self):
        acc = self.acc
        every = slice(None)
        self.first.recv(self.four_lines)
        self.last = self.quad(
            [
                (acc(self.zs[1], every, 0, 0), "z+"),
                (acc(self.zs[0], every, 0, 1), "z-"),
                (acc(every, self.ys[1], 1, 0), "y+"),
                (acc(every, self.ys[0], 1, 1), "y-"),
            ]
        )

    def neighbours(self):
        every = slice(None)
        self.second.recv(self.four_lines)
        self.to_partner(self.zs[0], every, every, self.ys[0])
        self.to_partner(self.zs[1], every, every, self.ys[1])

    def opposite(self):
        every = slice(None)
        self.last.recv(self.four_lines)
        self.to_partner(self.zs[2], every, every, self.ys[2])

    def finish(self):
        self.cross.recv(self.crossed)


class Waves(Plane):
    def both_ways(self, ya, za, yb, zb):
        a, b = self.acc(za, ya, 0, None), self.acc(zb, yb, 1, None)
        return self.quad([(a, "z+"), (a, "z-"), (b, "y+"), (b, "y-")])

    def onward(self, wave, yy, zz):
        acc = self.acc
        wave.recv(self.four)
        self.ends.append((yy, zz))
        self.lasts.append(
            self.quad(
                [
                    (acc(self.zs[1], yy, 0, 0), "z+"),
                    (acc(self.zs[0], yy, 0, 1), "z-"),
                    (acc(zz, self.ys[1], 1, 0), "y+"),
                    (acc(zz, self.ys[0], 1, 1), "y-"),
                ]
            )
        )
        for i in (0, 1):
            self.to_partner(self.zs[i], yy, zz, self.ys[i])

    def start(self):
        self.ends, self.lasts = [], []
        self.own_piece()
        self.wave0 = self.both_ways(self.y, self.z, self.y, self.z)
        self.to_partner(self.z, self.y, self.z, self.y)

    def step1(self):
        self.own_piece_on()
        self.waves1 = [
            self.both_ways(self.ys[i], self.z, self.y, self.zs[i]) for i in (0, 1)
        ]
        for i in (0, 1):
            self.to_partner(self.z, self.ys[i], self.zs[i], self.y)
        self.onward(self.wave0, self.y, self.z)

    def step2(self):
        self.far.recv(self.four_subs)
        self.wave2 = self.both_ways(self.ys[2], self.z, self.y, self.zs[2])
        self.to_partner(self.z, self.ys[2], self.zs[2], self.y)

    def step2_on(self):
        for i in (0, 1):
            self.onward(self.waves1[i], self.ys[i], self.zs[i])

    def step3(self):
        self.onward(self.wave2, self.ys[2], self.zs[2])
        self.ended(0)

    def ended(self, i):
        yy, zz = self.ends[i]
        self.lasts[i].recv(self.four_subs)
        self.to_partner(self.zs[2], yy, zz, self.ys[2])

    def opposite(self):
        for i in (1, 2, 3):
            self.ended(i)


def layer_kernel(
    total,
    res_hbm,
    q_hbm,
    kv_hbm,
    sink_hbm,
    ow_hbm,
    g1_hbm,
    b1_hbm,
    up_hbm,
    dn_hbm,
    g2_hbm,
    b2_hbm,
    out_ref,
    q_ref,
    kv_ref,
    res_ref,
    bias_ref,
    att_ref,
    afull_ref,
    wo_ref,
    wu_ref,
    wd_ref,
    pre_ref,
    tok_ref,
    act_ref,
    part_ref,
    rin_ref,
    fin_ref,
    g1_ref,
    b1_ref,
    g2_ref,
    b2_ref,
    sink_ref,
    loc_sem,
    send_sem,
    recv_sem,
):
    sp = lax.axis_index("sp")
    x = lax.axis_index("tp")
    z, y, c = sp // 8, lax.rem(sp // 2, 4), lax.rem(sp, 2)
    right, left, opp = lax.rem(x + 1, 4), lax.rem(x + 3, 4), lax.rem(x + 2, 4)

    def at(zz, yy, cc):
        return {"sp": zz * 8 + yy * 2 + cc, "tp": x}

    where_to = {
        "y+": at(z, lax.rem(y + 1, 4), c),
        "y-": at(z, lax.rem(y + 3, 4), c),
        "z+": at(lax.rem(z + 1, 4), y, c),
        "z-": at(lax.rem(z + 3, 4), y, c),
        "core": at(z, y, 1 - c),
        "x+": {"sp": sp, "tp": right},
        "x-": {"sp": sp, "tp": left},
        "xx": {"sp": sp, "tp": opp},
        "next": {"sp": lax.rem(sp + 1, 32), "tp": x},
        "prev": {"sp": lax.rem(sp + 31, 32), "tp": x},
    }

    barrier = pltpu.get_barrier_semaphore()
    for device in where_to.values():
        pl.semaphore_signal(barrier, inc=1, device_id=device, device_id_type=MESH)

    local = [
        pltpu.make_async_copy(ow_hbm, wo_ref.at[0], loc_sem.at[0]),
        pltpu.make_async_copy(kv_hbm, kv_ref.at[:, pl.ds(WINDOW, 1024)], loc_sem.at[1]),
        pltpu.make_async_copy(up_hbm, wu_ref.at[z, y, c], loc_sem.at[2]),
        pltpu.make_async_copy(dn_hbm, wd_ref.at[z, y, c], loc_sem.at[3]),
        pltpu.make_async_copy(q_hbm, q_ref, loc_sem.at[4]),
        pltpu.make_async_copy(res_hbm, res_ref, loc_sem.at[5]),
        pltpu.make_async_copy(sink_hbm, sink_ref, loc_sem.at[6]),
        pltpu.make_async_copy(g1_hbm, g1_ref, loc_sem.at[7]),
        pltpu.make_async_copy(b1_hbm, b1_ref, loc_sem.at[8]),
        pltpu.make_async_copy(g2_hbm, g2_ref, loc_sem.at[9]),
        pltpu.make_async_copy(b2_hbm, b2_ref, loc_sem.at[10]),
    ]
    for copy in local:
        copy.start()
    groups = []

    def link(index, src, dst, where):
        return pltpu.make_async_remote_copy(
            src_ref=src,
            dst_ref=dst,
            send_sem=send_sem.at[index],
            recv_sem=recv_sem.at[index],
            device_id=where_to[where],
            device_id_type=MESH,
        )

    def new_group():
        groups.append(Group(len(groups), link))
        return groups[-1]

    def send_to(src, dst, where):
        group = new_group()
        group.send(src, dst, where)
        return group

    def rows_of(ref):
        def acc(zz, yy, half, sub):
            low = half * 32 + (sub or 0) * 16
            return ref.at[zz, yy, c, pl.ds(low, 32 if sub is None else 16)]

        return acc

    def cols_of(zz, yy, half, sub):
        low = half * 768 + (sub or 0) * 384
        return wo_ref.at[pl.ds(1, 3), zz, yy, c, :, pl.ds(low, 768 if sub is None else 384)]

    def tail(slot, zz, depth):
        return wo_ref.at[slot, pl.ds(zz, depth), :, :, :, pl.ds(1536, 512)]

    def views_of(ref):
        return ref.at[0, 0], ref.at[0, 0, 0], ref.at[0, pl.ds(0, 2)], ref.at[:, :, 1 - c]

    def wo_view(width):
        return wo_ref.at[pl.ds(1, 3), 0, :, 0, :, pl.ds(0, width)]

    spread = pl.ds(0, 1536)
    crossed = wo_ref.at[pl.ds(1, 3), :, :, 1 - c, :, spread]
    out_w = Waves(new_group, cols_of, z, y, (wo_view(768), wo_view(384), None, crossed))
    up_w = Plane(new_group, rows_of(wu_ref), z, y, views_of(wu_ref))
    dn_w = Plane(new_group, rows_of(wd_ref), z, y, views_of(wd_ref))

    pl.semaphore_wait(barrier, len(where_to))
    local[0].wait()
    mine = wo_ref.at[0, z, y, c, :, spread]
    exchange = new_group()
    exchange.send(mine, wo_ref.at[3, z, y, c, :, spread], "x+")
    exchange.send(mine, wo_ref.at[1, z, y, c, :, spread], "x-")
    exchange.send(mine, wo_ref.at[2, z, y, c, :, spread], "xx")
    tails1, tails2, tails_on, tails_core = new_group(), new_group(), new_group(), new_group()
    tails1.send(tail(0, 2 * c, 1), tail(3, 2 * c, 1), "x+")
    tails1.send(tail(0, 2 * c + 1, 1), tail(1, 2 * c + 1, 1), "x-")
    tails2.send(tail(0, 2 * c + 1, 1), tail(3, 2 * c + 1, 1), "x+")
    tails2.send(tail(0, 2 * c, 1), tail(1, 2 * c, 1), "x-")
    local[1].wait()
    halo = new_group()
    halo.send(kv_ref.at[:, pl.ds(1024, 128)], kv_ref.at[:, pl.ds(0, 128)], "next")
    halo.send(kv_ref.at[:, pl.ds(128, 128)], kv_ref.at[:, pl.ds(1152, 128)], "prev")
    local[2].wait()
    up_w.own_piece()
    local[3].wait()
    dn_w.own_piece()
    exchange.recv(wo_ref.at[pl.ds(1, 3), z, y, c, :, spread])
    out_w.start()
    local[4].wait()
    local[6].wait()
    halo.recv(kv_ref.at[:, pl.ds(0, 256)])

    low_lanes = lax.broadcasted_iota(jnp.int32, (128, 128), 1) < 64
    low_keys = lax.broadcasted_iota(jnp.int32, (384, 128), 1) < 64
    first_head = lax.broadcasted_iota(jnp.int32, (256, 1), 0) < 128

    def attend_block(start, dst_ref, dst_row):
        row = lax.broadcasted_iota(jnp.int32, (128, 384), 0)
        col = lax.broadcasted_iota(jnp.int32, (128, 384), 1)
        key_pos = sp * 1024 + start - WINDOW + col
        valid = (col >= row) & (col <= row + 2 * WINDOW) & (key_pos >= 0) & (key_pos < total)
        bias_ref[...] = jnp.where(valid, 0.0, -1e30)
        for g in range(4):
            query = q_ref[pl.ds(start, 128), g * 128 : (g + 1) * 128].astype(F32) * 0.125
            swapped = pltpu.roll(query, 64, 1)
            lanes = slice((g // 2) * 128, (g // 2) * 128 + 128)
            keys = kv_ref[0, pl.ds(start, 384), lanes]
            values = kv_ref[1, pl.ds(start, 384), lanes]
            ones = jnp.ones_like(values)
            if g % 2 == 0:
                stacked = [jnp.where(low_lanes, query, 0.0), jnp.where(low_lanes, swapped, 0.0)]
                values = jnp.where(low_keys, values, ones)
            else:
                stacked = [jnp.where(low_lanes, 0.0, swapped), jnp.where(low_lanes, 0.0, query)]
                values = jnp.where(low_keys, ones, values)
            stacked = jnp.concatenate(stacked, axis=0).astype(BF16)
            scores = lax.dot_general(
                stacked, keys, (((1,), (1,)), ((), ())), preferred_element_type=F32
            )
            bias = bias_ref[...]
            scores = scores + jnp.concatenate([bias, bias], axis=0)
            sink = jnp.where(first_head, sink_ref[2 * g], sink_ref[2 * g + 1])
            top = jnp.maximum(jnp.max(scores, axis=1, keepdims=True), sink)
            weights = jnp.exp(scores - top).astype(BF16)
            rest = jnp.exp(sink - top)
            mixed = jnp.dot(weights, values, preferred_element_type=F32)
            a, b = mixed[:128], mixed[128:]
            a_swapped, b_swapped = pltpu.roll(a, 64, 1), pltpu.roll(b, 64, 1)
            if g % 2 == 0:
                num = jnp.where(low_lanes, a, b_swapped)
                den = jnp.where(low_lanes, a_swapped, b)
            else:
                num = jnp.where(low_lanes, a_swapped, b)
                den = jnp.where(low_lanes, a, b_swapped)
            den = den + jnp.where(low_lanes, rest[:128], rest[128:])
            dst_ref[pl.ds(dst_row, 128), g * 128 : (g + 1) * 128] = (num / den).astype(BF16)

    def attend_quarter(owner, dst_ref):
        @pl.loop(0, 2)
        def _(i):
            row = pl.multiple_of(i * 128, 128)
            attend_block(pl.multiple_of(owner * 256 + row, 128), dst_ref, row)

    mixes = new_group()
    attend_quarter(opp, att_ref.at[0])
    tails1.recv(tail(3, 0, 2))
    tails_on.send(tail(3, 2 * c, 1), tail(2, 2 * c, 1), "x+")
    tails_on.send(tail(1, 2 * c + 1, 1), tail(2, 2 * c + 1, 1), "x-")
    mixes.send(att_ref.at[0], afull_ref.at[:, pl.ds(1024, 512)], "xx")
    up_w.own_piece_on()
    dn_w.own_piece_on()
    attend_quarter(right, att_ref.at[1])
    mixes.send(att_ref.at[1], afull_ref.at[:, pl.ds(1536, 512)], "x+")
    out_w.step1()
    attend_quarter(left, att_ref.at[2])
    mixes.send(att_ref.at[2], afull_ref.at[:, pl.ds(512, 512)], "x-")
    out_w.step2()
    tails2.recv(tail(3, 0, 2))
    tails_core.same(tail(3, 2 * c, 2), "core")
    tails_core.same(tail(1, 2 * c, 2), "core")
    attend_quarter(x, afull_ref.at[:, pl.ds(0, 512)])
    out_w.step2_on()
    local[5].wait()
    for copy in local[7:]:
        copy.wait()

    @pl.loop(0, 4)
    def _(n):
        cols = pl.ds(pl.multiple_of(n * 512, 512), 512)
        pre_ref[:, cols] = res_ref[:, cols].astype(F32) + jnp.dot(
            afull_ref[:, 0:512],
            wo_ref[0, :, :, :, :, cols].reshape(512, 512),
            preferred_element_type=F32,
        )

    def project(cols):
        pre_ref[:, cols] += jnp.dot(
            afull_ref[:, 512:2048],
            wo_ref[1:4, :, :, :, :, cols].reshape(1536, 512),
            preferred_element_type=F32,
        )

    out_w.step3()
    tails_on.recv(tail(2, 0, 2))
    tails_core.same(tail(2, 2 * c, 2), "core")
    out_w.opposite()
    up_w.line()
    mixes.recv(att_ref)
    tails_core.recv(wo_ref.at[pl.ds(1, 3), pl.ds(2 - 2 * c, 2), :, :, :, pl.ds(1536, 512)])
    project(pl.ds(1536, 512))
    out_w.finish()

    @pl.loop(0, 3)
    def _(n):
        project(pl.ds(pl.multiple_of(n * 512, 512), 512))

    def first_norm(part):
        @pl.loop(0, 2)
        def _(i):
            rows = pl.ds(pl.multiple_of(part * 128 + i * 64, 64), 64)
            tok_ref[0, rows, :] = norm_rows(pre_ref[rows, :], g1_ref[...], b1_ref[...])

    top, bottom = pl.ds(0, 128), pl.ds(128, 128)
    first_norm(0)
    top_right = send_to(tok_ref.at[0, top], tok_ref.at[3, top], "x+")
    first_norm(1)
    bottom_left = send_to(tok_ref.at[0, bottom], tok_ref.at[1, bottom], "x-")
    others = new_group()
    others.send(tok_ref.at[0, bottom], tok_ref.at[3, bottom], "x+")
    others.send(tok_ref.at[0, top], tok_ref.at[1, top], "x-")

    def up_project(block, get_rows):
        @pl.loop(0, 4)
        def _(n):
            cols = pl.ds(pl.multiple_of(n * 512, 512), 512)
            weight = wu_ref[:, :, :, :, cols].reshape(2048, 512)
            hidden = jnp.dot(get_rows(), weight, preferred_element_type=F32)
            act_ref[block, :, cols] = jnp.square(jnp.maximum(hidden, 0.0)).astype(BF16)

    def down_project(block, dst_ref):
        @pl.loop(0, 4)
        def _(n):
            cols = pl.ds(pl.multiple_of(n * 512, 512), 512)
            weight = wd_ref[n].reshape(512, 2048)
            dst_ref[:, cols] = lax.dot_general(
                act_ref[block], weight, (((1,), (1,)), ((), ())), preferred_element_type=F32
            ).astype(dst_ref.dtype)

    def two_halves(left_rows, right_rows):
        return lambda: jnp.concatenate([tok_ref[3, left_rows, :], tok_ref[1, right_rows, :]], axis=0)

    up_w.line_on()
    dn_w.line()
    onward = new_group()
    top_right.recv(tok_ref.at[3, top])
    onward.send(tok_ref.at[3, top], tok_ref.at[2, top], "x+")
    bottom_left.recv(tok_ref.at[1, bottom])
    onward.send(tok_ref.at[1, bottom], tok_ref.at[2, bottom], "x-")
    up_w.neighbours()
    up_w.opposite()
    up_w.finish()
    up_project(0, two_halves(top, bottom))
    dn_w.line_on()
    up_project(3, lambda: tok_ref[0])
    dn_w.neighbours()
    others.recv(tok_ref.at[3])
    up_project(2, two_halves(bottom, top))
    dn_w.opposite()
    dn_w.finish()
    pure = new_group()
    for n in range(4):
        cols = pl.ds(n * 512, 512)
        part_ref[0, :, cols] = lax.dot_general(
            act_ref[0],
            wd_ref[n].reshape(512, 2048),
            (((1,), (1,)), ((), ())),
            preferred_element_type=F32,
        ).astype(BF16)
        pure.send(part_ref.at[0, top, cols], fin_ref.at[1, top, cols], "x-")
        pure.send(part_ref.at[0, bottom, cols], fin_ref.at[0, bottom, cols], "x+")
    onward.recv(tok_ref.at[2])
    up_project(1, lambda: tok_ref[2])
    down_project(1, part_ref.at[2])
    far = [new_group() for _ in range(CHUNKS)]
    rows = 128 // CHUNKS
    for i in range(CHUNKS):
        upper, lower = pl.ds(i * rows, rows), pl.ds(128 + i * rows, rows)
        far[i].send(part_ref.at[2, upper], rin_ref.at[1, upper], "x+")
        far[i].send(part_ref.at[2, lower], rin_ref.at[0, upper], "x-")
    down_project(2, part_ref.at[1])
    down_project(3, pre_ref)
    sums = [new_group() for _ in range(CHUNKS)]
    for i in range(CHUNKS):
        upper, lower = pl.ds(i * rows, rows), pl.ds(128 + i * rows, rows)
        far[i].recv(rin_ref.at[0, pl.ds(0, 2 * rows)])
        part_ref[1, lower, :] = (
            part_ref[1, lower, :].astype(F32) + rin_ref[1, upper, :].astype(F32)
        ).astype(BF16)
        sums[i].send(part_ref.at[1, lower], fin_ref.at[0, upper], "x+")
        part_ref[1, upper, :] = (
            part_ref[1, upper, :].astype(F32) + rin_ref[0, upper, :].astype(F32)
        ).astype(BF16)
        sums[i].send(part_ref.at[1, upper], fin_ref.at[1, lower], "x-")

    def finish_rows(low):
        part = pl.ds(low, rows)
        branch = pre_ref[part, :] + fin_ref[0, part, :].astype(F32) + fin_ref[1, part, :].astype(F32)
        out_ref[part, :] = norm_rows(tok_ref[0, part, :].astype(F32) + branch, g2_ref[...], b2_ref[...])

    pure.recv(fin_ref.at[0])
    for i in range(CHUNKS):
        sums[i].recv(fin_ref.at[0, pl.ds(0, 2 * rows)])
        finish_rows(i * rows)
        finish_rows(128 + i * rows)
    for group in groups:
        group.sent()


def on_device(
    residual_in,
    queries,
    keys_values,
    sink_logit,
    out_weight,
    norm1_gain,
    norm1_bias,
    up_weight,
    down_weight,
    norm2_gain,
    norm2_bias,
):
    total = queries.shape[0] * lax.axis_size("sp")
    any_spec = pl.BlockSpec(memory_space=pl.ANY)
    vmem = pl.BlockSpec(memory_space=pltpu.VMEM)
    row = lambda v: v.reshape(1, -1)
    return pl.pallas_call(
        functools.partial(layer_kernel, total),
        out_shape=pltpu.VMEM(residual_in.shape, BF16),
        in_specs=[any_spec] * 11,
        out_specs=vmem,
        scratch_shapes=[
            pltpu.VMEM((1024, 512), BF16),
            pltpu.VMEM((2, 1280, 256), BF16),
            pltpu.VMEM((256, 2048), BF16),
            pltpu.VMEM((128, 384), F32),
            pltpu.VMEM((3, 256, 512), BF16),
            pltpu.VMEM((256, 2048), BF16),
            pltpu.VMEM((4, 4, 4, 2, 16, 2048), BF16),
            pltpu.VMEM((4, 4, 2, 64, 2048), BF16),
            pltpu.VMEM((4, 4, 2, 64, 2048), BF16),
            pltpu.VMEM((256, 2048), F32),
            pltpu.VMEM((4, 256, 2048), BF16),
            pltpu.VMEM((4, 256, 2048), BF16),
            pltpu.VMEM((3, 256, 2048), BF16),
            pltpu.VMEM((2, 128, 2048), BF16),
            pltpu.VMEM((2, 256, 2048), BF16),
            pltpu.VMEM((1, 2048), F32),
            pltpu.VMEM((1, 2048), F32),
            pltpu.VMEM((1, 2048), F32),
            pltpu.VMEM((1, 2048), F32),
            pltpu.SMEM((8,), F32),
            pltpu.SemaphoreType.DMA((11,)),
            pltpu.SemaphoreType.DMA((N_COPIES,)),
            pltpu.SemaphoreType.DMA((N_COPIES,)),
        ],
        compiler_params=pltpu.CompilerParams(
            collective_id=0, has_side_effects=True, vmem_limit_bytes=58 * 1024 * 1024
        ),
        name="layer",
    )(
        residual_in,
        queries,
        keys_values,
        sink_logit,
        out_weight.reshape(4, 4, 2, 16, 2048),
        row(norm1_gain),
        row(norm1_bias),
        up_weight,
        down_weight.T,
        row(norm2_gain),
        row(norm2_bias),
    )


def solution(mesh):
    return jax.shard_map(
        on_device,
        mesh=mesh,
        in_specs=(
            P(("sp", "tp"), None),
            P("sp", "tp"),
            P(None, "sp", "tp"),
            P("tp"),
            P("tp", None),
            P(),
            P(),
            P("sp", "tp"),
            P("tp", "sp"),
            P(),
            P(),
        ),
        out_specs=P(("sp", "tp"), None),
        check_vma=False,
    )
```

time: 115 us -> 109 us (0.948)
  Pallas kernels: 114 us -> 108 us
    pallas_call x1, Pallas kernels: 114 us -> 108 us  [on_device(): pl.pallas_call(functools.partial(layer_kernel, total), out_shape=pltpu.VM...]
where the time goes in v3:
time: 109 us
  Pallas kernels  108 us (99%)
    pallas_call x1, Pallas kernels, on_device(): pl.pallas_call(functools.partial(layer_kernel, total), out_shape=pltpu.VM...  108 us

profile of v3, /device:TPU:1, one launch (start us, length us, event | category | flops | bytes accessed | tf_op | source)
XLA Modules:
  0.0 109.2 jit_solution(15557378316250881808)
XLA Ops:
  0.0 108.3 %layer.1 = bf16[256,2048]{1,0:T(8,128)(2,1)S(1)} custom-call(bf16[256,2048]{1,0:T(8,128)(2,1)} %res_hbm.1, bf16[1024,512]{1,0:T(8,128)(2,1)} %q_hbm.1, bf16[2,1024,256]{2,1,0:T(8,128)(2,1)} %kv_hbm.1, f32[8]{0:T(128)} %sink_hbm.1, bf16[4,4,2,16,2048]{4,3,2,1,0:T(8,128)(2,1)} %bitcast.6, f32[1,2048]{1,0:T(1,128)} %bitcast.8, f32[1,2048]{1,0:T(1,128)} %bitcast.9, ...), custom_call_target="tpu_custom_call" | custom-call | tf_op jit(solution)/shard_map/layer/pallas_call | solution.py:563
  108.3 1.0 copy.13
